TPU v7x, 32 devices: a whole 2x2x4 slice. The times are simulated.
32 devices in a mesh: sp: 16 (over z, y, x), tp: 2 (over core).
Axes of the slice: x: 2, y: 2, z: 4, core: 2. Of those that a mesh axis runs over, the one named last changes fastest.
Arguments:
- residual: bfloat16 [6144, 2048], P('sp'), may hold values from -6 to 6
- queries: bfloat16 [6144, 2048], P('sp', 'tp'), may hold values from -48 to 48
- keys: bfloat16 [6144, 2048], P('sp', 'tp'), may hold values from -48 to 48
- values: bfloat16 [6144, 2048], P('sp', 'tp'), may hold values from -6 to 6
- gate_cache: float32 [6144, 32], P('sp', 'tp'), may hold values from -1544 to 0, as said below
- doc_ids: int32 [6144], P('sp'), may hold values from 0 to 7, never falling along the last dimension, each value on 1 to 1536 neighbouring positions
- out_weight: bfloat16 [2048, 2048], P('tp'), may hold values from -1 to 1
- mix_gain: float32 [2048], replicated, may hold values from 0.1 to 1.9
- gate_weight: bfloat16 [2048, 5120], P('sp', 'tp'), may hold values from -0.125 to 0.125
- up_weight: bfloat16 [2048, 5120], P('sp', 'tp'), may hold values from -0.125 to 0.125
- down_weight: bfloat16 [5120, 2048], P('tp', 'sp'), may hold values from -0.15625 to 0.15625
Outputs:
- layer_out: bfloat16 [6144, 2048], P(('sp', 'tp'))
Inputs may be any that keep to these rules, and one draw needn't show every extreme that they name: `doc_ids`: positions of one document are consecutive; each document has 1 to 1536 positions, and one has exactly that many. `gate_cache`: no column rises from one position to the next.
All inputs are finite; a program needn't handle non-finite values.
Results may differ from a plain program's by a relative error of at most 0.018.
Values may be sent and summed in bfloat16 or wider, within the bound.
A program may use at most 128 MiB of HBM per device.

v0:
```python
import jax
import jax.numpy as jnp
from jax import lax
from jax.sharding import PartitionSpec as P

REACH = 4
EPSILON = 1e-06
NEGATIVE = -1e30


def from_behind(value, axis, steps):
    count = lax.axis_size(axis)
    first, last = (max(0, -steps), min(count, count - steps))
    return lax.ppermute(value, axis, [(source, source + steps) for source in range(first, last)])


def normalize(middle, gain):
    widened = middle.astype(jnp.float32)
    factor = lax.rsqrt(jnp.mean(widened * widened, axis=-1, keepdims=True) + EPSILON)
    return (widened * factor * gain).astype(jnp.bfloat16)


def local(
    residual,
    queries,
    keys,
    values,
    gate_cache,
    doc_ids,
    out_weight,
    mix_gain,
    gate_weight,
    up_weight,
    down_weight,
):
    tok_rows = queries.shape[0]
    heads_here = gate_cache.shape[1]
    head_size = queries.shape[1] // heads_here
    sp_index = lax.axis_index("sp")
    key_parts = [keys]
    value_parts = [values]
    cache_parts = [gate_cache]
    doc_parts = [doc_ids]
    for distance in range(1, REACH + 1):
        moved_keys, moved_values = from_behind((keys, values), "sp", distance)
        moved_cache, moved_docs = from_behind((gate_cache, doc_ids), "sp", distance)
        key_parts.append(moved_keys)
        value_parts.append(moved_values)
        cache_parts.append(moved_cache)
        doc_parts.append(moved_docs)
    all_keys = jnp.concatenate(key_parts[::-1], axis=0)
    all_values = jnp.concatenate(value_parts[::-1], axis=0)
    all_cache = jnp.concatenate(cache_parts[::-1], axis=0)
    all_docs = jnp.concatenate(doc_parts[::-1], axis=0)
    key_count = all_keys.shape[0]
    query_pos = sp_index * tok_rows + jnp.arange(tok_rows, dtype=jnp.int32)
    key_pos = (sp_index - REACH) * tok_rows + jnp.arange(key_count, dtype=jnp.int32)
    visible = (
        (key_pos[None, :] <= query_pos[:, None])
        & (key_pos[None, :] >= 0)
        & (all_docs[None, :] == doc_ids[:, None])
    )
    query_heads = queries.reshape(tok_rows, heads_here, head_size)
    key_heads = all_keys.reshape(key_count, heads_here, head_size)
    value_heads = all_values.reshape(key_count, heads_here, head_size)
    score_scale = head_size ** (-0.5)
    scores = (
        jnp.einsum("qhd,khd->hqk", query_heads, key_heads, preferred_element_type=jnp.float32)
        * score_scale
    )
    scores = scores + gate_cache.T[:, :, None] - all_cache.T[:, None, :]
    scores = jnp.where(visible[None], scores, NEGATIVE)
    row_max = jnp.max(scores, axis=-1, keepdims=True)
    exp_scores = jnp.exp(scores - row_max)
    weights = (exp_scores / jnp.sum(exp_scores, axis=-1, keepdims=True)).astype(jnp.bfloat16)
    attended = jnp.einsum("hqk,khd->qhd", weights, value_heads, preferred_element_type=jnp.float32)
    attended = attended.astype(jnp.bfloat16).reshape(tok_rows, heads_here * head_size)
    row_share = tok_rows // lax.axis_size("tp")
    tp_index = lax.axis_index("tp")
    partial_value = jnp.dot(attended, out_weight, preferred_element_type=jnp.float32)
    attn_sum = lax.psum(partial_value.astype(jnp.bfloat16), "tp").astype(jnp.float32)
    whole_middle = (residual.astype(jnp.float32) + attn_sum).astype(jnp.bfloat16)
    mixer_in = normalize(whole_middle, mix_gain)
    middle = lax.dynamic_slice_in_dim(whole_middle, tp_index * row_share, row_share, 0)
    held_gate, held_up = (
        lax.all_gather(gate_weight, "sp", axis=0, tiled=True),
        lax.all_gather(up_weight, "sp", axis=0, tiled=True),
    )
    gate_proj = jnp.dot(mixer_in, held_gate, preferred_element_type=jnp.float32)
    up_proj = jnp.dot(mixer_in, held_up, preferred_element_type=jnp.float32)
    hidden = (jax.nn.silu(gate_proj) * up_proj).astype(jnp.bfloat16)
    partials = jnp.dot(
        hidden,
        lax.all_gather(down_weight, "sp", axis=1, tiled=True),
        preferred_element_type=jnp.float32,
    )
    down_sum = lax.psum_scatter(
        partials.astype(jnp.bfloat16), "tp", scatter_dimension=0, tiled=True
    ).astype(jnp.float32)
    return (middle.astype(jnp.float32) + down_sum).astype(jnp.bfloat16)


def solution(mesh):
    return jax.shard_map(
        local,
        mesh=mesh,
        in_specs=(
            P("sp", None),
            P("sp", "tp"),
            P("sp", "tp"),
            P("sp", "tp"),
            P("sp", "tp"),
            P("sp"),
            P("tp", None),
            P(),
            P("sp", "tp"),
            P("sp", "tp"),
            P("tp", "sp"),
        ),
        out_specs=P(("sp", "tp"), None),
        check_vma=False,
    )
```

profile of v0, /device:TPU:0, one launch (start us, length us, event | category | flops | bytes accessed | tf_op | source)
XLA Modules:
  0.0 706.5 jit_solution(17122347479193859977)
XLA Ops:
  7.4 5.1 collective-permute-start.4
  12.5 4.4 collective-permute-start.5
  16.8 3.4 collective-permute-start.6
  20.3 2.5 collective-permute-start.7
  22.8 3.5 collective-permute-start.8
  26.4 1.5 copy.18
  27.9 3.9 collective-permute-start.9
  31.8 3.4 collective-permute-start.10
  35.3 1.3 collective-permute-start.11
  36.6 1.8 collective-permute-start.12
  38.4 0.7 constant_dynamic-update-slice_fusion.16
  39.1 3.2 compare_and_fusion
  42.7 54.6 %collective-permute-start.13 = (f32[384,16]{0,1:T(8,128)}, f32[384,16]{0,1:T(8,128)S(1)}, u32[]{:S(2)}, u32[]{:S(2)}) collective-permute-start(f32[384,16]{0,1:T(8,128)} %param.15), channel_id=1, source_target_pairs={{0,6},{2,8},{4,10},{6,12},{8,14},{10,16},{12,18},{14,20},{16,22},{... | collective-permute-start | bytes 73736 | tf_op jit(solution)/shard_map/ppermute | solution.py:14
  97.3 1.7 collective-permute-done.13
  99.0 1.3 collective-permute-start.14
  100.3 1.7 collective-permute-done.14
  102.0 6.3 collective-permute-start.15
  108.3 1.7 collective-permute-done.15
  110.0 8.2 %collective-permute-start = (bf16[384,1024]{1,0:T(8,128)(2,1)}, bf16[384,1024]{1,0:T(8,128)(2,1)S(1)}, u32[]{:S(2)}, u32[]{:S(2)}) collective-permute-start(bf16[384,1024]{1,0:T(8,128)(2,1)} %param.14), channel_id=1, source_target_pairs={{0,8},{2,10},{4,12},{6,14},{8,16},{10,18},{12,20},{14,22},{16,24},... | collective-permute-start | bytes 2359304 | tf_op jit(solution)/shard_map/ppermute | solution.py:14
  118.3 0.7 constant_dynamic-update-slice_fusion.11
  119.0 3.1 collective-permute-start.1
  122.1 0.9 constant_dynamic-update-slice_fusion.10
  123.0 2.8 collective-permute-start.2
  125.8 1.0 constant_dynamic-update-slice_fusion.9
  126.8 2.8 collective-permute-start.3
  129.6 0.9 constant_dynamic-update-slice_fusion.8
  130.5 0.9 constant_dynamic-update-slice_fusion.7
  131.4 0.9 constant_dynamic-update-slice_fusion.6
  132.4 6.3 copy.17
  138.7 0.9 constant_dynamic-update-slice_fusion.4
  139.6 2.1 constant_dynamic-update-slice_fusion.3
  141.7 11.9 %collective-permute-done.2 = bf16[384,1024]{1,0:T(8,128)(2,1)S(1)} collective-permute-done((bf16[384,1024]{1,0:T(8,128)(2,1)S(1)}, bf16[384,1024]{1,0:T(8,128)(2,1)S(1)}, u32[]{:S(2)}, u32[]{:S(2)}) %collective-permute-start.2) | collective-permute-done | bytes 786464 | tf_op jit(solution)/shard_map/ppermute | solution.py:14
  153.7 0.9 constant_dynamic-update-slice_fusion.2
  154.6 2.1 constant_dynamic-update-slice_fusion.1
  156.7 0.9 constant_dynamic-update-slice_fusion
  157.6 6.4 copy.16
  164.1 26.9 %fusion.22 = (f32[16,384]{1,0:T(8,128)S(1)}, f32[16,384,1920]{1,2,0:T(8,128)}) fusion(f32[16,1920]{1,0:T(8,128)S(1)} %bitcast.33, f32[16,384]{1,0:T(8,128)S(1)} %bitcast.32, pred[384,1920]{0,1:T(8,128)(4,1)S(1)} %copy-done.3, bf16[1920,16,64]{0,2,1:T(8,128)(2,1)} %bitcast.29, bf16[384,16,64]{0,2,1:T(8,128)(2,1)S(1)} %bitcast.31), kind=kOutput, calls=%fused_computation.53 | convolution fusion | flops 1580730240 | bytes 52813824 | tf_op jit(solution)/shard_map/sub | solution.py:74
  190.9 17.4 %fusion.14 = bf16[16,64,384]{2,1,0:T(8,128)(2,1)S(1)} fusion(bf16[1920,16,64]{0,2,1:T(8,128)(2,1)} %bitcast.30, f32[16,384,1920]{1,2,0:T(8,128)} %get-tuple-element.8, f32[16,384]{1,0:T(8,128)S(1)} %get-tuple-element.7), kind=kOutput, calls=%fused_computation.24 | convolution fusion | flops 1533935616 | bytes 51929088 | tf_op jit(solution)/shard_map/hqk,khd->qhd/dot_general | solution.py:76
  208.3 3.0 convolution_convert_fusion
  213.4 43.0 %all-reduce.2.cloned.1.call-done = bf16[384,2048]{1,0:T(8,128)(2,1)} async-done(((bf16[384,2048]{1,0:T(8,128)(2,1)}), bf16[384,2048]{1,0:T(8,128)(2,1)}) %all-reduce.2.cloned.1.call-update) | async-done | bytes 1572880 | tf_op jit(solution)/shard_map/psum | solution.py:81
  256.3 2.1 fusion.11
  258.5 111.8 %all-gather.4.cloned.1.call-done = bf16[2048,2560]{1,0:T(8,128)(2,1)} async-done(((bf16[128,2560]{1,0:T(8,128)(2,1)}), bf16[2048,2560]{1,0:T(8,128)(2,1)}) %all-gather.4.cloned.1.call-update) | async-done | bytes 10485776 | tf_op jit(solution)/shard_map/all_gather | solution.py:86
  370.3 8.9 %fusion.17 = f32[384,2560]{1,0:T(8,128)} fusion(bf16[2048,2560]{1,0:T(8,128)(2,1)} %all-gather.4.cloned.1.call-done, bf16[384,2048]{1,0:T(8,128)(2,1)S(1)} %get-tuple-element.6, f32[2048]{0:T(1024)S(1)} %copy-done.6, f32[384]{0:T(512)S(1)} %add_rsqrt_fusion), kind=kOutput, calls=%fused_computation.25 | convolution fusion | flops 4029677568 | bytes 16000512 | tf_op jit(solution)/shard_map/dot_general | solution.py:89
  379.2 123.1 %all-gather.6.cloned.1.call-done = bf16[2048,2560]{1,0:T(8,128)(2,1)} async-done(((bf16[128,2560]{1,0:T(8,128)(2,1)}), bf16[2048,2560]{1,0:T(8,128)(2,1)}) %all-gather.6.cloned.1.call-update) | async-done | bytes 10485776 | tf_op jit(solution)/shard_map/all_gather | solution.py:87
  502.3 169.3 %all-gather.8.cloned.1.call-done = bf16[2560,2048]{1,0:T(8,128)(2,1)} async-done(((bf16[2560,128]{1,0:T(8,128)(2,1)}), bf16[2560,2048]{1,0:T(8,128)(2,1)}) %all-gather.8.cloned.1.call-update) | async-done | bytes 10485776 | tf_op jit(solution)/shard_map/all_gather | solution.py:94
  671.5 17.7 %convolution_convert_fusion.1 = bf16[384,2048]{1,0:T(8,128)(2,1)} fusion(bf16[2560,2048]{1,0:T(8,128)(2,1)} %all-gather.8.cloned.1.call-done, bf16[2048,2560]{1,0:T(8,128)(2,1)} %all-gather.6.cloned.1.call-done, f32[384,2560]{1,0:T(8,128)} %fusion.17, bf16[384,2048]{1,0:T(8,128)(2,1)S(1)} %get-tuple-element.6, f32[2048]{0:T(1024)S(1)} %copy-done.6, ...), kind=kOutput, calls=%fused_computation.22 | convolution fusion | flops 8062894080 | bytes 28059136 | tf_op jit(solution)/shard_map/dot_general | solution.py:92
  689.3 7.4 %reduce-scatter.2.cloned.1.call-done = bf16[192,2048]{1,0:T(8,128)(2,1)} async-done(((bf16[384,2048]{1,0:T(8,128)(2,1)}), bf16[192,2048]{1,0:T(8,128)(2,1)}) %reduce-scatter.2.cloned.1.call-update) | async-done | bytes 786448 | tf_op jit(solution)/shard_map/reduce_scatter | solution.py:97
  696.7 2.3 add_convert_fusion.1
  (49 shorter events, 2.4 us)
Async XLA Ops:
  7.4 115.6 %copy-start.2 = (bf16[384,1024]{1,0:T(8,128)(2,1)S(1)}, bf16[384,1024]{1,0:T(8,128)(2,1)}, u32[]{:S(2)}) copy-start(bf16[384,1024]{1,0:T(8,128)(2,1)} %param.14) | copy-start | bytes 2359300
  7.4 249.0 %all-reduce.2.cloned.1.call-start = ((), (), s32[]{:S(2)}) async-start(), calls=%async_computation.1 | async-start | bytes 3145728 | tf_op jit(solution)/shard_map/psum | solution.py:81
  7.4 20.5 %collective-permute-start.4 = (s32[384]{0:T(512)}, s32[384]{0:T(512)S(1)}, u32[]{:S(2)}, u32[]{:S(2)}) collective-permute-start(s32[384]{0:T(512)} %param.16), channel_id=1, source_target_pairs={{0,8},{2,10},{4,12},{6,14},{8,16},{10,18},{12,20},{14,22},{16,24},... | collective-permute-start | bytes 4616 | tf_op jit(solution)/shard_map/ppermute | solution.py:14
  12.5 19.4 %collective-permute-start.5 = (s32[384]{0:T(512)}, s32[384]{0:T(512)S(1)}, u32[]{:S(2)}, u32[]{:S(2)}) collective-permute-start(s32[384]{0:T(512)} %param.16), channel_id=1, source_target_pairs={{0,6},{2,8},{4,10},{6,12},{8,14},{10,16},{12,18},{14,20},{16,22},{... | collective-permute-start | bytes 4616 | tf_op jit(solution)/shard_map/ppermute | solution.py:14
  16.8 18.4 %collective-permute-start.6 = (s32[384]{0:T(512)}, s32[384]{0:T(512)S(1)}, u32[]{:S(2)}, u32[]{:S(2)}) collective-permute-start(s32[384]{0:T(512)} %param.16), channel_id=1, source_target_pairs={{0,4},{2,6},{4,8},{6,10},{8,12},{10,14},{12,16},{14,18},{16,20},{1... | collective-permute-start | bytes 4616 | tf_op jit(solution)/shard_map/ppermute | solution.py:14
  20.3 16.4 %collective-permute-start.7 = (s32[384]{0:T(512)}, s32[384]{0:T(512)S(1)}, u32[]{:S(2)}, u32[]{:S(2)}) collective-permute-start(s32[384]{0:T(512)} %param.16), channel_id=1, source_target_pairs={{0,2},{2,4},{4,6},{6,8},{8,10},{10,12},{12,14},{14,16},{16,18},{18... | collective-permute-start | bytes 4616 | tf_op jit(solution)/shard_map/ppermute | solution.py:14
  22.8 96.2 %collective-permute-start.8 = (bf16[384,1024]{1,0:T(8,128)(2,1)}, bf16[384,1024]{1,0:T(8,128)(2,1)S(1)}, u32[]{:S(2)}, u32[]{:S(2)}) collective-permute-start(bf16[384,1024]{1,0:T(8,128)(2,1)} %param.13), channel_id=1, source_target_pairs={{0,8},{2,10},{4,12},{6,14},{8,16},{10,18},{12,20},{14,22},{16,24},... | collective-permute-start | bytes 2359304 | tf_op jit(solution)/shard_map/ppermute | solution.py:14
  27.9 103.6 %copy-start.1 = (bf16[384,1024]{1,0:T(8,128)(2,1)S(1)}, bf16[384,1024]{1,0:T(8,128)(2,1)}, u32[]{:S(2)}) copy-start(bf16[384,1024]{1,0:T(8,128)(2,1)} %param.13) | copy-start | bytes 2359300
  27.9 95.1 %collective-permute-start.9 = (bf16[384,1024]{1,0:T(8,128)(2,1)}, bf16[384,1024]{1,0:T(8,128)(2,1)S(1)}, u32[]{:S(2)}, u32[]{:S(2)}) collective-permute-start(bf16[384,1024]{1,0:T(8,128)(2,1)} %param.13), channel_id=1, source_target_pairs={{0,6},{2,8},{4,10},{6,12},{8,14},{10,16},{12,18},{14,20},{16,22},{... | collective-permute-start | bytes 2359304 | tf_op jit(solution)/shard_map/ppermute | solution.py:14
  31.8 94.9 %collective-permute-start.10 = (bf16[384,1024]{1,0:T(8,128)(2,1)}, bf16[384,1024]{1,0:T(8,128)(2,1)S(1)}, u32[]{:S(2)}, u32[]{:S(2)}) collective-permute-start(bf16[384,1024]{1,0:T(8,128)(2,1)} %param.13), channel_id=1, source_target_pairs={{0,4},{2,6},{4,8},{6,10},{8,12},{10,14},{12,16},{14,18},{16,20},{1... | collective-permute-start | bytes 2359304 | tf_op jit(solution)/shard_map/ppermute | solution.py:14
  35.3 95.2 %collective-permute-start.11 = (bf16[384,1024]{1,0:T(8,128)(2,1)}, bf16[384,1024]{1,0:T(8,128)(2,1)S(1)}, u32[]{:S(2)}, u32[]{:S(2)}) collective-permute-start(bf16[384,1024]{1,0:T(8,128)(2,1)} %param.13), channel_id=1, source_target_pairs={{0,2},{2,4},{4,6},{6,8},{8,10},{10,12},{12,14},{14,16},{16,18},{18... | collective-permute-start | bytes 2359304 | tf_op jit(solution)/shard_map/ppermute | solution.py:14
  36.6 6.0 collective-permute-start.12
  42.7 56.3 %collective-permute-start.13 = (f32[384,16]{0,1:T(8,128)}, f32[384,16]{0,1:T(8,128)S(1)}, u32[]{:S(2)}, u32[]{:S(2)}) collective-permute-start(f32[384,16]{0,1:T(8,128)} %param.15), channel_id=1, source_target_pairs={{0,6},{2,8},{4,10},{6,12},{8,14},{10,16},{12,18},{14,20},{16,22},{... | collective-permute-start | bytes 73736 | tf_op jit(solution)/shard_map/ppermute | solution.py:14
  99.0 3.0 collective-permute-start.14
  102.0 8.0 %collective-permute-start.15 = (f32[384,16]{0,1:T(8,128)}, f32[384,16]{0,1:T(8,128)S(1)}, u32[]{:S(2)}, u32[]{:S(2)}) collective-permute-start(f32[384,16]{0,1:T(8,128)} %param.15), channel_id=1, source_target_pairs={{0,2},{2,4},{4,6},{6,8},{8,10},{10,12},{12,14},{14,16},{16,18},{18... | collective-permute-start | bytes 73736 | tf_op jit(solution)/shard_map/ppermute | solution.py:14
  110.0 28.7 %collective-permute-start = (bf16[384,1024]{1,0:T(8,128)(2,1)}, bf16[384,1024]{1,0:T(8,128)(2,1)S(1)}, u32[]{:S(2)}, u32[]{:S(2)}) collective-permute-start(bf16[384,1024]{1,0:T(8,128)(2,1)} %param.14), channel_id=1, source_target_pairs={{0,8},{2,10},{4,12},{6,14},{8,16},{10,18},{12,20},{14,22},{16,24},... | collective-permute-start | bytes 2359304 | tf_op jit(solution)/shard_map/ppermute | solution.py:14
  119.0 20.6 %collective-permute-start.1 = (bf16[384,1024]{1,0:T(8,128)(2,1)}, bf16[384,1024]{1,0:T(8,128)(2,1)}, u32[]{:S(2)}, u32[]{:S(2)}) collective-permute-start(bf16[384,1024]{1,0:T(8,128)(2,1)} %param.14), channel_id=1, source_target_pairs={{0,6},{2,8},{4,10},{6,12},{8,14},{10,16},{12,18},{14,20},{16,22},{... | collective-permute-start | bytes 2359304 | tf_op jit(solution)/shard_map/ppermute | solution.py:14
  123.0 30.7 %collective-permute-start.2 = (bf16[384,1024]{1,0:T(8,128)(2,1)S(1)}, bf16[384,1024]{1,0:T(8,128)(2,1)S(1)}, u32[]{:S(2)}, u32[]{:S(2)}) collective-permute-start(bf16[384,1024]{1,0:T(8,128)(2,1)S(1)} %copy-done.2), channel_id=1, source_target_pairs={{0,4},{2,6},{4,8},{6,10},{8,12},{10,14},{12,16},{14,18},{16,20},{1... | collective-permute-start | bytes 2359304 | tf_op jit(solution)/shard_map/ppermute | solution.py:14
  126.8 27.8 %collective-permute-start.3 = (bf16[384,1024]{1,0:T(8,128)(2,1)S(1)}, bf16[384,1024]{1,0:T(8,128)(2,1)}, u32[]{:S(2)}, u32[]{:S(2)}) collective-permute-start(bf16[384,1024]{1,0:T(8,128)(2,1)S(1)} %copy-done.2), channel_id=1, source_target_pairs={{0,2},{2,4},{4,6},{6,8},{8,10},{10,12},{12,14},{14,16},{16,18},{18... | collective-permute-start | bytes 2359304 | tf_op jit(solution)/shard_map/ppermute | solution.py:14
  157.6 6.4 copy-start.3
  157.6 6.4 copy-start.4
  190.9 17.4 %copy-start.5 = (bf16[1024,2048]{1,0:T(8,128)(2,1)S(1)}, bf16[1024,2048]{1,0:T(8,128)(2,1)}, u32[]{:S(2)}) copy-start(bf16[1024,2048]{1,0:T(8,128)(2,1)} %param.17) | copy-start | bytes 12582916
  211.4 45.0 %copy-start = (bf16[384,2048]{1,0:T(8,128)(2,1)S(1)}, bf16[384,2048]{1,0:T(8,128)(2,1)}, u32[]{:S(2)}) copy-start(bf16[384,2048]{1,0:T(8,128)(2,1)} %param.11) | copy-start | bytes 4718596
  211.4 158.9 %copy-start.6 = (f32[2048]{0:T(1024)S(1)}, f32[2048]{0:T(1024)}, u32[]{:S(2)}) copy-start(f32[2048]{0:T(1024)} %param.18) | copy-start | bytes 24580
  211.4 158.9 %all-gather.4.cloned.1.call-start = ((), (), s32[]{:S(2)}) async-start(), calls=%async_computation.2 | async-start | bytes 11141120 | tf_op jit(solution)/shard_map/all_gather | solution.py:86
  212.0 290.3 %all-gather.6.cloned.1.call-start = ((), (), s32[]{:S(2)}) async-start(), calls=%async_computation.3 | async-start | bytes 11141120 | tf_op jit(solution)/shard_map/all_gather | solution.py:87
  212.6 459.0 %all-gather.8.cloned.1.call-start = ((), (), s32[]{:S(2)}) async-start(), calls=%async_computation.4 | async-start | bytes 11141120 | tf_op jit(solution)/shard_map/all_gather | solution.py:94
  213.1 483.5 %reduce-scatter.2.cloned.1.call-start = ((), (), s32[]{:S(2)}) async-start(), calls=%async_computation.5 | async-start | bytes 2359296 | tf_op jit(solution)/shard_map/reduce_scatter | solution.py:97
Sparse Core Ops, SparseCore 0:
  211.5 44.7 all-reduce.1
  689.4 7.2 reduce-scatter.1
Sparse Core Ops, SparseCore 1:
  214.6 155.6 all-gather.3
  372.8 129.4 all-gather.5
  504.9 166.6 all-gather.7
where the time goes:
time: 708 us; the launch traced here: 707 us
  waiting for transfers between devices  473 us (67%)
  starting transfers between devices  109 us (15%)
  matrix products  73.9 us (10%)
  local copies, waits for them, and re-layouts  27.4 us (4%)
  between operations  15.3 us (2%)
  other arithmetic  7.69 us (1%)
    all_gather x1, waiting for transfers between devices, local(): lax.all_gather(down_weight, 'sp', axis=1, tiled=True)  169 us
    all_gather x1, waiting for transfers between devices, local(): lax.all_gather(up_weight, 'sp', axis=0, tiled=True)  123 us
    all_gather x1, waiting for transfers between devices, local(): lax.all_gather(gate_weight, 'sp', axis=0, tiled=True)  112 us
    ppermute x16, starting transfers between devices, from_behind(): lax.ppermute(value, axis, [(source, source + steps) for source in range(f...  108 us
    psum x1, waiting for transfers between devices, local(): lax.psum(partial_value.astype(jnp.bfloat16), 'tp').astype(jnp.float32)  43 us
    sub x1, matrix products, local(): exp_scores = jnp.exp(scores - row_max)  26.9 us
    dot_general x1, matrix products, local(): jnp.dot(hidden, lax.all_gather(down_weight, 'sp', axis=1, tiled=True), pr...  17.7 us
    dot_general x1, matrix products, local(): jnp.einsum('hqk,khd->qhd', weights, value_heads, preferred_element_type=j...  17.4 us
  transfers between devices with their start and end apart: 21, of which 10 were waited for; matrix products, arithmetic and copies ran while one was open for 5% of the time, Pallas kernels for 0%

commit v1 on v0

--- a/solution.py
+++ b/solution.py
@@ -91,7 +91,7 @@
     hidden = (jax.nn.silu(gate_proj) * up_proj).astype(jnp.bfloat16)
     partials = jnp.dot(
         hidden,
-        lax.all_gather(down_weight, "sp", axis=1, tiled=True),
+        jnp.concatenate(lax.all_gather(down_weight, "sp"), axis=1),
         preferred_element_type=jnp.float32,
     )
     down_sum = lax.psum_scatter(

time: 708 us -> 671 us (0.948)
  waiting for transfers between devices: 473 us -> 422 us
  local copies, waits for them, and re-layouts: 27.4 us -> 41.5 us
    all_gather x1, waiting for transfers between devices: 169 us -> 112 us  [local(): lax.all_gather(down_weight, 'sp')]
    reshape x0 -> x1, local copies, waits for them, and re-layouts: none -> 14.1 us  [local(): jnp.concatenate(lax.all_gather(down_weight, 'sp'), axis=1)]
  transfers between devices with their start and end apart: 21 -> 21, of which waited for: 10 -> 10; matrix products, arithmetic and copies ran while one was open for 5% -> 7% of each run, Pallas kernels for 0% -> 0%
where the time goes in v1:
time: 671 us; the launch traced here: 669 us
  waiting for transfers between devices  422 us (63%)
  starting transfers between devices  109 us (16%)
  matrix products  74 us (11%)
  local copies, waits for them, and re-layouts  41.5 us (6%)
  between operations  15.3 us (2%)
  other arithmetic  7.69 us (1%)
    all_gather x1, waiting for transfers between devices, local(): lax.all_gather(up_weight, 'sp', axis=0, tiled=True)  123 us
    all_gather x1, waiting for transfers between devices, local(): lax.all_gather(gate_weight, 'sp', axis=0, tiled=True)  118 us
    all_gather x1, waiting for transfers between devices, local(): lax.all_gather(down_weight, 'sp')  112 us
    ppermute x16, starting transfers between devices, from_behind(): lax.ppermute(value, axis, [(source, source + steps) for source in range(f...  108 us
    psum x1, waiting for transfers between devices, local(): lax.psum(partial_value.astype(jnp.bfloat16), 'tp').astype(jnp.float32)  43 us
    sub x1, matrix products, local(): exp_scores = jnp.exp(scores - row_max)  26.9 us
    dot_general x1, matrix products, local(): jnp.dot(hidden, jnp.concatenate(lax.all_gather(down_weight, 'sp'), axis=1...  17.7 us
    dot_general x1, matrix products, local(): jnp.einsum('hqk,khd->qhd', weights, value_heads, preferred_element_type=j...  17.4 us
  transfers between devices with their start and end apart: 21, of which 10 were waited for; matrix products, arithmetic and copies ran while one was open for 7% of the time, Pallas kernels for 0%

profile of v1, /device:TPU:0, one launch (start us, length us, event | category | flops | bytes accessed | tf_op | source)
XLA Modules:
  0.0 669.3 jit_solution(3138330263467673049)
XLA Ops:
  7.4 5.1 collective-permute-start.4
  12.5 4.4 collective-permute-start.5
  16.8 3.4 collective-permute-start.6
  20.3 2.5 collective-permute-start.7
  22.8 3.5 collective-permute-start.8
  26.4 1.5 copy.22
  27.9 3.9 collective-permute-start.9
  31.8 3.4 collective-permute-start.10
  35.3 1.3 collective-permute-start.11
  36.6 1.8 collective-permute-start.12
  39.1 3.2 compare_and_fusion
  42.7 54.6 %collective-permute-start.13 = (f32[384,16]{0,1:T(8,128)}, f32[384,16]{0,1:T(8,128)S(1)}, u32[]{:S(2)}, u32[]{:S(2)}) collective-permute-start(f32[384,16]{0,1:T(8,128)} %param.15), channel_id=1, source_target_pairs={{0,6},{2,8},{4,10},{6,12},{8,14},{10,16},{12,18},{14,20},{16,22},{... | collective-permute-start | bytes 73736 | tf_op jit(solution)/shard_map/ppermute | solution.py:14
  97.3 1.7 collective-permute-done.13
  99.0 1.3 collective-permute-start.14
  100.3 1.7 collective-permute-done.14
  102.0 6.3 collective-permute-start.15
  108.3 1.7 collective-permute-done.15
  110.0 8.2 %collective-permute-start = (bf16[384,1024]{1,0:T(8,128)(2,1)}, bf16[384,1024]{1,0:T(8,128)(2,1)S(1)}, u32[]{:S(2)}, u32[]{:S(2)}) collective-permute-start(bf16[384,1024]{1,0:T(8,128)(2,1)} %param.14), channel_id=1, source_target_pairs={{0,8},{2,10},{4,12},{6,14},{8,16},{10,18},{12,20},{14,22},{16,24},... | collective-permute-start | bytes 2359304 | tf_op jit(solution)/shard_map/ppermute | solution.py:14
  118.3 0.7 constant_dynamic-update-slice_fusion.11
  119.0 3.1 collective-permute-start.1
  122.1 0.9 constant_dynamic-update-slice_fusion.10
  123.0 2.8 collective-permute-start.2
  125.8 1.0 constant_dynamic-update-slice_fusion.9
  126.8 2.8 collective-permute-start.3
  129.6 0.9 constant_dynamic-update-slice_fusion.8
  130.5 0.9 constant_dynamic-update-slice_fusion.7
  131.4 0.9 constant_dynamic-update-slice_fusion.6
  132.4 6.3 copy.21
  138.7 0.9 constant_dynamic-update-slice_fusion.4
  139.6 2.1 constant_dynamic-update-slice_fusion.3
  141.7 11.9 %collective-permute-done.2 = bf16[384,1024]{1,0:T(8,128)(2,1)S(1)} collective-permute-done((bf16[384,1024]{1,0:T(8,128)(2,1)S(1)}, bf16[384,1024]{1,0:T(8,128)(2,1)S(1)}, u32[]{:S(2)}, u32[]{:S(2)}) %collective-permute-start.2) | collective-permute-done | bytes 786464 | tf_op jit(solution)/shard_map/ppermute | solution.py:14
  153.7 0.9 constant_dynamic-update-slice_fusion.2
  154.6 2.1 constant_dynamic-update-slice_fusion.1
  156.7 0.9 constant_dynamic-update-slice_fusion
  157.6 6.4 copy.20
  164.1 26.9 %fusion.22 = (f32[16,384]{1,0:T(8,128)S(1)}, f32[16,384,1920]{1,2,0:T(8,128)}) fusion(f32[16,1920]{1,0:T(8,128)S(1)} %bitcast.39, f32[16,384]{1,0:T(8,128)S(1)} %bitcast.38, pred[384,1920]{0,1:T(8,128)(4,1)S(1)} %copy-done.3, bf16[1920,16,64]{0,2,1:T(8,128)(2,1)} %bitcast.35, bf16[384,16,64]{0,2,1:T(8,128)(2,1)S(1)} %bitcast.37), kind=kOutput, calls=%fused_computation.53 | convolution fusion | flops 1580730240 | bytes 52813824 | tf_op jit(solution)/shard_map/sub | solution.py:74
  190.9 17.4 %fusion.14 = bf16[16,64,384]{2,1,0:T(8,128)(2,1)S(1)} fusion(bf16[1920,16,64]{0,2,1:T(8,128)(2,1)} %bitcast.36, f32[16,384,1920]{1,2,0:T(8,128)} %get-tuple-element.8, f32[16,384]{1,0:T(8,128)S(1)} %get-tuple-element.7), kind=kOutput, calls=%fused_computation.24 | convolution fusion | flops 1533935616 | bytes 51929088 | tf_op jit(solution)/shard_map/hqk,khd->qhd/dot_general | solution.py:76
  208.3 3.0 convolution_convert_fusion
  213.4 43.0 %all-reduce.2.cloned.1.call-done = bf16[384,2048]{1,0:T(8,128)(2,1)} async-done(((bf16[384,2048]{1,0:T(8,128)(2,1)}), bf16[384,2048]{1,0:T(8,128)(2,1)}) %all-reduce.2.cloned.1.call-update) | async-done | bytes 1572880 | tf_op jit(solution)/shard_map/psum | solution.py:81
  256.3 2.1 fusion.11
  258.5 111.8 %all-gather.9.cloned.1.call-done = bf16[40960,128]{1,0:T(8,128)(2,1)} async-done(((bf16[2560,128]{1,0:T(8,128)(2,1)}), bf16[40960,128]{1,0:T(8,128)(2,1)}) %all-gather.9.cloned.1.call-update) | async-done | bytes 10485776 | tf_op jit(solution)/shard_map/all_gather | solution.py:94
  370.3 14.1 %copy.24 = bf16[2560,16,128]{0,2,1:T(8,128)(2,1)} copy(bf16[2560,16,128]{2,0,1:T(8,128)(2,1)} %bitcast.33) | data formatting | bytes 20971520 | tf_op jit(solution)/shard_map/reshape | solution.py:94
  384.3 117.9 %all-gather.5.cloned.1.call-done = bf16[2048,2560]{1,0:T(8,128)(2,1)} async-done(((bf16[128,2560]{1,0:T(8,128)(2,1)}), bf16[2048,2560]{1,0:T(8,128)(2,1)}) %all-gather.5.cloned.1.call-update) | async-done | bytes 10485776 | tf_op jit(solution)/shard_map/all_gather | solution.py:86
  502.3 8.9 %fusion.17 = f32[384,2560]{1,0:T(8,128)} fusion(bf16[2048,2560]{1,0:T(8,128)(2,1)} %all-gather.5.cloned.1.call-done, bf16[384,2048]{1,0:T(8,128)(2,1)S(1)} %get-tuple-element.6, f32[2048]{0:T(1024)S(1)} %copy-done.6, f32[384]{0:T(512)S(1)} %add_rsqrt_fusion), kind=kOutput, calls=%fused_computation.25 | convolution fusion | flops 4029677568 | bytes 16000512 | tf_op jit(solution)/shard_map/dot_general | solution.py:89
  511.2 123.1 %all-gather.7.cloned.1.call-done = bf16[2048,2560]{1,0:T(8,128)(2,1)} async-done(((bf16[128,2560]{1,0:T(8,128)(2,1)}), bf16[2048,2560]{1,0:T(8,128)(2,1)}) %all-gather.7.cloned.1.call-update) | async-done | bytes 10485776 | tf_op jit(solution)/shard_map/all_gather | solution.py:87
  634.3 17.7 %convolution_convert_fusion.1 = bf16[384,2048]{1,0:T(8,128)(2,1)} fusion(bf16[2560,2048]{0,1:T(8,128)(2,1)} %bitcast.34, bf16[2048,2560]{1,0:T(8,128)(2,1)} %all-gather.7.cloned.1.call-done, f32[384,2560]{1,0:T(8,128)} %fusion.17, bf16[384,2048]{1,0:T(8,128)(2,1)S(1)} %get-tuple-element.6, f32[2048]{0:T(1024)S(1)} %copy-done.6, f32[384]{0:T(512)S(1)} %add_rsqrt_fusion), kind=kOutput, calls=%fused_computation.22 | convolution fusion | flops 8062894080 | bytes 28059136 | tf_op jit(solution)/shard_map/dot_general | solution.py:92
  652.1 7.4 %reduce-scatter.2.cloned.1.call-done = bf16[192,2048]{1,0:T(8,128)(2,1)} async-done(((bf16[384,2048]{1,0:T(8,128)(2,1)}), bf16[192,2048]{1,0:T(8,128)(2,1)}) %reduce-scatter.2.cloned.1.call-update) | async-done | bytes 786448 | tf_op jit(solution)/shard_map/reduce_scatter | solution.py:97
  659.5 2.3 add_convert_fusion.1
  (50 shorter events, 3.1 us)
Async XLA Ops:
  7.4 115.6 %copy-start.2 = (bf16[384,1024]{1,0:T(8,128)(2,1)S(1)}, bf16[384,1024]{1,0:T(8,128)(2,1)}, u32[]{:S(2)}) copy-start(bf16[384,1024]{1,0:T(8,128)(2,1)} %param.14) | copy-start | bytes 2359300
  7.4 249.0 %all-reduce.2.cloned.1.call-start = ((), (), s32[]{:S(2)}) async-start(), calls=%async_computation.1 | async-start | bytes 3145728 | tf_op jit(solution)/shard_map/psum | solution.py:81
  7.4 20.5 %collective-permute-start.4 = (s32[384]{0:T(512)}, s32[384]{0:T(512)S(1)}, u32[]{:S(2)}, u32[]{:S(2)}) collective-permute-start(s32[384]{0:T(512)} %param.16), channel_id=1, source_target_pairs={{0,8},{2,10},{4,12},{6,14},{8,16},{10,18},{12,20},{14,22},{16,24},... | collective-permute-start | bytes 4616 | tf_op jit(solution)/shard_map/ppermute | solution.py:14
  12.5 19.4 %collective-permute-start.5 = (s32[384]{0:T(512)}, s32[384]{0:T(512)S(1)}, u32[]{:S(2)}, u32[]{:S(2)}) collective-permute-start(s32[384]{0:T(512)} %param.16), channel_id=1, source_target_pairs={{0,6},{2,8},{4,10},{6,12},{8,14},{10,16},{12,18},{14,20},{16,22},{... | collective-permute-start | bytes 4616 | tf_op jit(solution)/shard_map/ppermute | solution.py:14
  16.8 18.4 %collective-permute-start.6 = (s32[384]{0:T(512)}, s32[384]{0:T(512)S(1)}, u32[]{:S(2)}, u32[]{:S(2)}) collective-permute-start(s32[384]{0:T(512)} %param.16), channel_id=1, source_target_pairs={{0,4},{2,6},{4,8},{6,10},{8,12},{10,14},{12,16},{14,18},{16,20},{1... | collective-permute-start | bytes 4616 | tf_op jit(solution)/shard_map/ppermute | solution.py:14
  20.3 16.4 %collective-permute-start.7 = (s32[384]{0:T(512)}, s32[384]{0:T(512)S(1)}, u32[]{:S(2)}, u32[]{:S(2)}) collective-permute-start(s32[384]{0:T(512)} %param.16), channel_id=1, source_target_pairs={{0,2},{2,4},{4,6},{6,8},{8,10},{10,12},{12,14},{14,16},{16,18},{18... | collective-permute-start | bytes 4616 | tf_op jit(solution)/shard_map/ppermute | solution.py:14
  22.8 96.2 %collective-permute-start.8 = (bf16[384,1024]{1,0:T(8,128)(2,1)}, bf16[384,1024]{1,0:T(8,128)(2,1)S(1)}, u32[]{:S(2)}, u32[]{:S(2)}) collective-permute-start(bf16[384,1024]{1,0:T(8,128)(2,1)} %param.13), channel_id=1, source_target_pairs={{0,8},{2,10},{4,12},{6,14},{8,16},{10,18},{12,20},{14,22},{16,24},... | collective-permute-start | bytes 2359304 | tf_op jit(solution)/shard_map/ppermute | solution.py:14
  27.9 103.6 %copy-start.1 = (bf16[384,1024]{1,0:T(8,128)(2,1)S(1)}, bf16[384,1024]{1,0:T(8,128)(2,1)}, u32[]{:S(2)}) copy-start(bf16[384,1024]{1,0:T(8,128)(2,1)} %param.13) | copy-start | bytes 2359300
  27.9 95.1 %collective-permute-start.9 = (bf16[384,1024]{1,0:T(8,128)(2,1)}, bf16[384,1024]{1,0:T(8,128)(2,1)S(1)}, u32[]{:S(2)}, u32[]{:S(2)}) collective-permute-start(bf16[384,1024]{1,0:T(8,128)(2,1)} %param.13), channel_id=1, source_target_pairs={{0,6},{2,8},{4,10},{6,12},{8,14},{10,16},{12,18},{14,20},{16,22},{... | collective-permute-start | bytes 2359304 | tf_op jit(solution)/shard_map/ppermute | solution.py:14
  31.8 94.9 %collective-permute-start.10 = (bf16[384,1024]{1,0:T(8,128)(2,1)}, bf16[384,1024]{1,0:T(8,128)(2,1)S(1)}, u32[]{:S(2)}, u32[]{:S(2)}) collective-permute-start(bf16[384,1024]{1,0:T(8,128)(2,1)} %param.13), channel_id=1, source_target_pairs={{0,4},{2,6},{4,8},{6,10},{8,12},{10,14},{12,16},{14,18},{16,20},{1... | collective-permute-start | bytes 2359304 | tf_op jit(solution)/shard_map/ppermute | solution.py:14
  35.3 95.2 %collective-permute-start.11 = (bf16[384,1024]{1,0:T(8,128)(2,1)}, bf16[384,1024]{1,0:T(8,128)(2,1)S(1)}, u32[]{:S(2)}, u32[]{:S(2)}) collective-permute-start(bf16[384,1024]{1,0:T(8,128)(2,1)} %param.13), channel_id=1, source_target_pairs={{0,2},{2,4},{4,6},{6,8},{8,10},{10,12},{12,14},{14,16},{16,18},{18... | collective-permute-start | bytes 2359304 | tf_op jit(solution)/shard_map/ppermute | solution.py:14
  36.6 6.0 collective-permute-start.12
  42.7 56.3 %collective-permute-start.13 = (f32[384,16]{0,1:T(8,128)}, f32[384,16]{0,1:T(8,128)S(1)}, u32[]{:S(2)}, u32[]{:S(2)}) collective-permute-start(f32[384,16]{0,1:T(8,128)} %param.15), channel_id=1, source_target_pairs={{0,6},{2,8},{4,10},{6,12},{8,14},{10,16},{12,18},{14,20},{16,22},{... | collective-permute-start | bytes 73736 | tf_op jit(solution)/shard_map/ppermute | solution.py:14
  99.0 3.0 collective-permute-start.14
  102.0 8.0 %collective-permute-start.15 = (f32[384,16]{0,1:T(8,128)}, f32[384,16]{0,1:T(8,128)S(1)}, u32[]{:S(2)}, u32[]{:S(2)}) collective-permute-start(f32[384,16]{0,1:T(8,128)} %param.15), channel_id=1, source_target_pairs={{0,2},{2,4},{4,6},{6,8},{8,10},{10,12},{12,14},{14,16},{16,18},{18... | collective-permute-start | bytes 73736 | tf_op jit(solution)/shard_map/ppermute | solution.py:14
  110.0 28.7 %collective-permute-start = (bf16[384,1024]{1,0:T(8,128)(2,1)}, bf16[384,1024]{1,0:T(8,128)(2,1)S(1)}, u32[]{:S(2)}, u32[]{:S(2)}) collective-permute-start(bf16[384,1024]{1,0:T(8,128)(2,1)} %param.14), channel_id=1, source_target_pairs={{0,8},{2,10},{4,12},{6,14},{8,16},{10,18},{12,20},{14,22},{16,24},... | collective-permute-start | bytes 2359304 | tf_op jit(solution)/shard_map/ppermute | solution.py:14
  119.0 20.6 %collective-permute-start.1 = (bf16[384,1024]{1,0:T(8,128)(2,1)}, bf16[384,1024]{1,0:T(8,128)(2,1)}, u32[]{:S(2)}, u32[]{:S(2)}) collective-permute-start(bf16[384,1024]{1,0:T(8,128)(2,1)} %param.14), channel_id=1, source_target_pairs={{0,6},{2,8},{4,10},{6,12},{8,14},{10,16},{12,18},{14,20},{16,22},{... | collective-permute-start | bytes 2359304 | tf_op jit(solution)/shard_map/ppermute | solution.py:14
  123.0 30.7 %collective-permute-start.2 = (bf16[384,1024]{1,0:T(8,128)(2,1)S(1)}, bf16[384,1024]{1,0:T(8,128)(2,1)S(1)}, u32[]{:S(2)}, u32[]{:S(2)}) collective-permute-start(bf16[384,1024]{1,0:T(8,128)(2,1)S(1)} %copy-done.2), channel_id=1, source_target_pairs={{0,4},{2,6},{4,8},{6,10},{8,12},{10,14},{12,16},{14,18},{16,20},{1... | collective-permute-start | bytes 2359304 | tf_op jit(solution)/shard_map/ppermute | solution.py:14
  126.8 27.8 %collective-permute-start.3 = (bf16[384,1024]{1,0:T(8,128)(2,1)S(1)}, bf16[384,1024]{1,0:T(8,128)(2,1)}, u32[]{:S(2)}, u32[]{:S(2)}) collective-permute-start(bf16[384,1024]{1,0:T(8,128)(2,1)S(1)} %copy-done.2), channel_id=1, source_target_pairs={{0,2},{2,4},{4,6},{6,8},{8,10},{10,12},{12,14},{14,16},{16,18},{18... | collective-permute-start | bytes 2359304 | tf_op jit(solution)/shard_map/ppermute | solution.py:14
  157.6 6.4 copy-start.3
  157.6 6.4 copy-start.4
  190.9 17.4 %copy-start.5 = (bf16[1024,2048]{1,0:T(8,128)(2,1)S(1)}, bf16[1024,2048]{1,0:T(8,128)(2,1)}, u32[]{:S(2)}) copy-start(bf16[1024,2048]{1,0:T(8,128)(2,1)} %param.17) | copy-start | bytes 12582916
  211.4 45.0 %copy-start = (bf16[384,2048]{1,0:T(8,128)(2,1)S(1)}, bf16[384,2048]{1,0:T(8,128)(2,1)}, u32[]{:S(2)}) copy-start(bf16[384,2048]{1,0:T(8,128)(2,1)} %param.11) | copy-start | bytes 4718596
  211.4 158.9 %all-gather.9.cloned.1.call-start = ((), (), s32[]{:S(2)}) async-start(), calls=%async_computation.5 | async-start | bytes 11141120 | tf_op jit(solution)/shard_map/all_gather | solution.py:94
  212.0 290.3 %all-gather.5.cloned.1.call-start = ((), (), s32[]{:S(2)}) async-start(), calls=%async_computation.2 | async-start | bytes 11141120 | tf_op jit(solution)/shard_map/all_gather | solution.py:86
  212.6 421.8 %all-gather.7.cloned.1.call-start = ((), (), s32[]{:S(2)}) async-start(), calls=%async_computation.3 | async-start | bytes 11141120 | tf_op jit(solution)/shard_map/all_gather | solution.py:87
  213.1 446.3 %reduce-scatter.2.cloned.1.call-start = ((), (), s32[]{:S(2)}) async-start(), calls=%async_computation.4 | async-start | bytes 2359296 | tf_op jit(solution)/shard_map/reduce_scatter | solution.py:97
  370.2 132.0 %copy-start.6 = (f32[2048]{0:T(1024)S(1)}, f32[2048]{0:T(1024)}, u32[]{:S(2)}) copy-start(f32[2048]{0:T(1024)} %param.18) | copy-start | bytes 24580
Sparse Core Ops, SparseCore 0:
  211.5 44.7 all-reduce.1
  652.2 7.2 reduce-scatter.1
Sparse Core Ops, SparseCore 1:
  214.6 155.6 all-gather.8
  372.8 129.4 all-gather.4
  504.9 129.4 all-gather.6
